TPU v7x, 32 devices: a whole 2x2x4 slice. The times are simulated.
32 devices in a mesh: sp: 4 (over y, x), tp: 8 (over z, core).
Axes of the slice: x: 2, y: 2, z: 4, core: 2. Of those that a mesh axis runs over, the one named last changes fastest.
Arguments:
- cotangent: bfloat16 [1024, 2048], P('sp', 'tp'), may hold values from -6 to 6
- block_input: bfloat16 [1024, 2048], P('sp', 'tp'), may hold values from -6 to 6
- routes: int32 [1024, 2], P('sp'), may hold values from 0 to 3, all different within a row; in each aligned block of 256 rows (0 to 255, 256 to 511, ...) at most 160 rows name the same one
- route_weights: float32 [1024, 2], P('sp'), may hold values from 0.1 to 0.9
- gate_weight: bfloat16 [4, 2048, 7168], P('sp', None, 'tp'), may hold values from -0.125 to 0.125
- up_weight: bfloat16 [4, 2048, 7168], P('sp', None, 'tp'), may hold values from -0.125 to 0.125
- down_weight: bfloat16 [4, 7168, 2048], P('sp', 'tp'), may hold values from -0.0625 to 0.0625
- out_weight: bfloat16 [1024, 2048], P('tp'), may hold values from -0.1875 to 0.1875
- conv_out: bfloat16 [1024, 1024], P('tp', 'sp'), may hold values from -6 to 6
- gate_pre: bfloat16 [1024, 1024], P('tp', 'sp'), may hold values from -6 to 6
- prior_states: bfloat16 [1024, 1024], P('tp', 'sp'), may hold values from -6 to 6
- recur_weight: bfloat16 [16, 64, 64], replicated, may hold values from -0.75 to 0.75
- input_gate_matrix: bfloat16 [16, 64, 64], replicated, may hold values from -0.75 to 0.75
- decay_param: float32 [1024], replicated, may hold values from 4 to 16
- decay_jump: float32 [1024, 1024], P('tp', 'sp'), may hold values from -1 to 0, as said below
Outputs:
- gate_weight_grad: bfloat16 [4, 2048, 7168], P('sp', None, 'tp')
- up_weight_grad: bfloat16 [4, 2048, 7168], P('sp', None, 'tp')
- down_weight_grad: bfloat16 [4, 7168, 2048], P('sp', 'tp')
- out_weight_grad: float32 [1024, 2048], P('tp', 'sp')
- conv_grad: bfloat16 [1024, 1024], P('tp', 'sp')
- valve_logit_derivative: bfloat16 [1024, 1024], P('tp', 'sp')
Inputs may be any that keep to these rules, and one draw needn't show every extreme that they name: In each aligned block of 256 rows (the rows of one index of sp) no expert is named by more than 160 routes, a bound that some block reaches; a row names 2 different experts. `decay_jump`: every entry is at most -1 / 20480.
All inputs are finite; a program needn't handle non-finite values.
Results may differ from a plain program's by a relative error of at most 0.018.
Values may be sent and summed in bfloat16 or wider, within the bound.
A program may use at most 128 MiB of HBM per device.

v0:
```python
import jax
import jax.numpy as jnp
from jax import lax
from jax.sharding import PartitionSpec as P

HEAD_DIM = 64
TOP_K = 2


RATE_SCALE = 8.0


def prefix(value, axis, join, neutral):
    count, mine = (lax.axis_size(axis), lax.axis_index(axis))
    pieces = jax.tree.map(lambda part: lax.all_gather(part, axis), value)
    pieces = jax.tree.map(lambda part: part[::-1], pieces)
    mine = count - 1 - mine
    so_far = jax.tree.map(
        lambda part, zero: jnp.full_like(part, 0) + jnp.asarray(zero, part.dtype), value, neutral
    )

    def turn(position, so_far):
        longer = join(so_far, jax.tree.map(lambda part: part[position], pieces))
        return jax.tree.map(lambda new, old: jnp.where(position < mine, new, old), longer, so_far)

    return lax.fori_loop(0, count - 1, turn, so_far)


def link_pairs(left_pair, right_pair):
    return (left_pair[0] * right_pair[0], right_pair[0] * left_pair[1] + right_pair[1])


def later_first(earlier_pair, later_pair):
    return (earlier_pair[0] * later_pair[0], later_pair[1] + later_pair[0] * earlier_pair[1])


def routing_tables(routes, experts, capacity):
    flat_routes = routes.reshape(-1)
    onehot = (flat_routes[:, None] == jnp.arange(experts, dtype=jnp.int32)[None, :]).astype(
        jnp.int32
    )
    slot_rank = jnp.sum((jnp.cumsum(onehot, axis=0) - onehot) * onehot, axis=1)
    target = (flat_routes * capacity + slot_rank).reshape(routes.shape[0], routes.shape[1])
    slot_ids = jnp.arange(experts * capacity, dtype=jnp.int32)
    return jnp.transpose(target)[:, None, :] == slot_ids[None, :, None]


def spread(placing, route_hits, rows_in, cot_in, route_weights):
    sent_rows = jnp.dot(placing, rows_in, preferred_element_type=jnp.float32).astype(jnp.bfloat16)
    scaled = (
        jnp.transpose(route_weights)[:, :, None] * cot_in.astype(jnp.float32)[None, :, :]
    ).astype(jnp.bfloat16)
    sent_cot = jnp.einsum(
        "kst,ktd->sd", route_hits, scaled, preferred_element_type=jnp.float32
    ).astype(jnp.bfloat16)
    return (sent_rows, sent_cot)


def expert_work(slot_rows, slot_cot, w_gate, w_up, w_down):
    minor = (((1,), (1,)), ((), ()))
    gate_act = jnp.dot(slot_rows, w_gate, preferred_element_type=jnp.float32)
    up_act = jnp.dot(slot_rows, w_up, preferred_element_type=jnp.float32)
    sigma_gate = jax.nn.sigmoid(gate_act)
    silu_val = gate_act * sigma_gate
    hidden = (silu_val * up_act).astype(jnp.bfloat16)
    d_hidden = lax.dot_general(slot_cot, w_down, minor, preferred_element_type=jnp.float32)
    d_gate = (d_hidden * up_act * sigma_gate * (1.0 + gate_act * (1.0 - sigma_gate))).astype(
        jnp.bfloat16
    )
    d_up = (d_hidden * silu_val).astype(jnp.bfloat16)
    width_part = lax.dot_general(d_gate, w_gate, minor, preferred_element_type=jnp.float32)
    width_part = width_part + lax.dot_general(d_up, w_up, minor, preferred_element_type=jnp.float32)
    return (hidden, d_gate, d_up, width_part)


def weight_grads(slot_rows, slot_cot, hidden, d_gate, d_up):
    major = (((0,), (0,)), ((), ()))
    gate_grad = lax.dot_general(
        slot_rows, d_gate, major, preferred_element_type=jnp.float32
    ).astype(jnp.bfloat16)
    up_grad = lax.dot_general(slot_rows, d_up, major, preferred_element_type=jnp.float32).astype(
        jnp.bfloat16
    )
    down_grad = lax.dot_general(hidden, slot_cot, major, preferred_element_type=jnp.float32).astype(
        jnp.bfloat16
    )
    return (gate_grad[None], up_grad[None], down_grad[None])


def local(
    cotangent,
    block_input,
    routes,
    route_weights,
    gate_weight,
    up_weight,
    down_weight,
    out_weight,
    conv_out,
    gate_pre,
    prior_states,
    recur_weight,
    input_gate_matrix,
    decay_param,
    decay_jump,
):
    experts = lax.axis_size("sp")
    tok_rows = cotangent.shape[0]
    capacity = 5 * tok_rows * TOP_K // (4 * experts)
    route_hits = routing_tables(routes, experts, capacity)
    placing = jnp.sum(route_hits.astype(jnp.int32), axis=0).astype(jnp.bfloat16)
    hit_table = route_hits.astype(jnp.bfloat16)
    sent_rows, sent_cot = spread(placing, hit_table, block_input, cotangent, route_weights)
    part_rows, portion_adjoint = (
        lax.all_to_all(
            sent_rows.reshape(experts, capacity, -1), "sp", split_axis=0, concat_axis=0, tiled=True
        ),
        lax.all_to_all(
            sent_cot.reshape(experts, capacity, -1), "sp", split_axis=0, concat_axis=0, tiled=True
        ),
    )
    got_rows, got_cot = (
        lax.all_gather(part_rows, "tp", axis=2, tiled=True),
        lax.all_gather(portion_adjoint, "tp", axis=2, tiled=True),
    )
    full_width = got_rows.shape[2]
    slot_rows = got_rows.reshape(-1, full_width)
    slot_cot = got_cot.reshape(-1, full_width)
    hidden, d_gate, d_up, width_part = expert_work(
        slot_rows, slot_cot, gate_weight[0], up_weight[0], down_weight[0]
    )
    gate_grad, up_grad, down_grad = weight_grads(slot_rows, slot_cot, hidden, d_gate, d_up)
    summed = lax.psum_scatter(
        width_part.reshape(experts, capacity, full_width).astype(jnp.bfloat16),
        "tp",
        scatter_dimension=2,
        tiled=True,
    )
    handed_result = lax.all_to_all(summed, "sp", split_axis=0, concat_axis=0, tiled=True).reshape(
        experts * capacity, -1
    )
    moe_grad = lax.dot_general(
        placing, handed_result, (((0,), (0,)), ((), ())), preferred_element_type=jnp.float32
    )
    block_grad = (cotangent.astype(jnp.float32) + moe_grad).astype(jnp.bfloat16)
    full_grad = lax.all_gather(block_grad, "tp", axis=1, tiled=True)
    channels = conv_out.shape[0]
    length = conv_out.shape[1]
    head_count = channels // HEAD_DIM
    head_start = lax.axis_index("tp") * head_count
    w_recur = lax.dynamic_slice_in_dim(recur_weight, head_start, head_count, 0)
    w_input = lax.dynamic_slice_in_dim(input_gate_matrix, head_start, head_count, 0)
    rate_parameter = lax.dynamic_slice_in_dim(decay_param, head_start * HEAD_DIM, channels, 0)[
        :, None
    ]
    shaped = conv_out.reshape(head_count, HEAD_DIM, length)
    recur_gate = jax.nn.sigmoid(
        jnp.einsum("hij,hit->hjt", w_recur, shaped, preferred_element_type=jnp.float32).reshape(
            channels, length
        )
    )
    input_gate = jax.nn.sigmoid(
        jnp.einsum("hij,hit->hjt", w_input, shaped, preferred_element_type=jnp.float32).reshape(
            channels, length
        )
    )
    softened = jax.nn.softplus(-rate_parameter)
    log_decay = -RATE_SCALE * recur_gate * softened + decay_jump
    decay_val = jnp.exp(log_decay)
    norm_scale = jnp.sqrt(-jnp.expm1(2.0 * log_decay))
    conv_vals = conv_out.astype(jnp.float32)
    prior_vals = prior_states.astype(jnp.float32)
    state = decay_val * prior_vals + norm_scale * input_gate * conv_vals
    gelu_val, gelu_pull = jax.vjp(jax.nn.gelu, gate_pre.astype(jnp.float32))
    mixed = (gelu_val * state).astype(jnp.bfloat16)
    d_mixed = lax.dot_general(
        out_weight, full_grad, (((1,), (1,)), ((), ())), preferred_element_type=jnp.float32
    )
    valve_logit_derivative = gelu_pull(d_mixed * state)[0].astype(jnp.bfloat16)
    d_state = d_mixed * gelu_val
    shifted = jnp.concatenate([decay_val[:, 1:], jnp.ones((channels, 1), jnp.float32)], axis=1)
    flipped = lax.associative_scan(link_pairs, (jnp.flip(shifted, 1), jnp.flip(d_state, 1)), axis=1)
    decay_prod = jnp.flip(flipped[0], 1)
    local_sum = jnp.flip(flipped[1], 1)
    summary = (decay_val[:, 0] * decay_prod[:, 0], decay_val[:, 0] * local_sum[:, 0])
    carried = prefix(
        summary,
        "sp",
        later_first,
        (jnp.ones((channels,), jnp.float32), jnp.zeros((channels,), jnp.float32)),
    )[1]
    state_grad = local_sum + decay_prod * carried[:, None]
    grad_log = (
        state_grad * prior_vals * decay_val
        - state_grad * input_gate * conv_vals * decay_val * decay_val / norm_scale
    )
    grad_recur = (grad_log * -RATE_SCALE * softened * recur_gate * (1.0 - recur_gate)).astype(
        jnp.bfloat16
    )
    grad_input = (state_grad * norm_scale * conv_vals * input_gate * (1.0 - input_gate)).astype(
        jnp.bfloat16
    )
    back_recur = jnp.einsum(
        "hij,hjt->hit",
        w_recur,
        grad_recur.reshape(head_count, HEAD_DIM, length),
        preferred_element_type=jnp.float32,
    ).reshape(channels, length)
    back_input = jnp.einsum(
        "hij,hjt->hit",
        w_input,
        grad_input.reshape(head_count, HEAD_DIM, length),
        preferred_element_type=jnp.float32,
    ).reshape(channels, length)
    conv_grad = (state_grad * norm_scale * input_gate + back_recur + back_input).astype(
        jnp.bfloat16
    )
    projected = lax.psum_scatter(
        lax.dot_general(
            full_grad, mixed, (((0,), (1,)), ((), ())), preferred_element_type=jnp.float32
        ).astype(jnp.bfloat16),
        "sp",
        scatter_dimension=0,
        tiled=True,
    ).astype(jnp.float32)
    out_weight_grad = jnp.transpose(projected)
    return (gate_grad, up_grad, down_grad, out_weight_grad, conv_grad, valve_logit_derivative)


def solution(mesh):
    in_specs = (
        P("sp", "tp"),
        P("sp", "tp"),
        P("sp", None),
        P("sp", None),
        P("sp", None, "tp"),
        P("sp", None, "tp"),
        P("sp", "tp", None),
        P("tp", None),
        P("tp", "sp"),
        P("tp", "sp"),
        P("tp", "sp"),
        P(),
        P(),
        P(),
        P("tp", "sp"),
    )
    out_specs = (
        P("sp", None, "tp"),
        P("sp", None, "tp"),
        P("sp", "tp", None),
        P("tp", "sp"),
        P("tp", "sp"),
        P("tp", "sp"),
    )
    return jax.shard_map(local, mesh=mesh, in_specs=in_specs, out_specs=out_specs, check_vma=False)
```

profile of v0, /device:TPU:0, one launch (start us, length us, event | category | flops | bytes accessed | tf_op | source)
XLA Modules:
  0.0 229.2 jit_solution(16892057116044407689)
XLA Ops:
  8.4 1.2 reduce-window.6
  11.3 1.1 convolution_convert_fusion.1
  12.5 11.7 %all_to_all.15 = bf16[4,160,256]{2,1,0:T(8,128)(2,1)} all-to-all(bf16[4,160,256]{2,1,0:T(8,128)(2,1)S(1)} %bitcast.101), channel_id=1, replica_groups=mesh['sp'=4,'tp'=8] {'sp'}, dimensions={0} | all-to-all | bytes 655360 | tf_op jit(solution)/shard_map/all_to_all | solution.py:115
  24.8 9.3 %all_to_all.16 = bf16[4,160,256]{2,1,0:T(8,128)(2,1)} all-to-all(bf16[4,160,256]{2,1,0:T(8,128)(2,1)S(1)} %bitcast.104), channel_id=1, replica_groups=mesh['sp'=4,'tp'=8] {'sp'}, dimensions={0} | all-to-all | bytes 655360 | tf_op jit(solution)/shard_map/all_to_all | solution.py:118
  34.2 24.6 %all-gather.6.cloned.1.call-done = bf16[4,160,2048]{2,1,0:T(8,128)(2,1)} async-done(((bf16[4,160,256]{2,1,0:T(8,128)(2,1)}), bf16[4,160,2048]{2,1,0:T(8,128)(2,1)}) %all-gather.6.cloned.1.call-update) | async-done | bytes 2621456 | tf_op jit(solution)/shard_map/all_gather | solution.py:123
  58.8 7.2 %fusion.3 = f32[640,896]{1,0:T(8,128)} fusion(bf16[640,2048]{1,0:T(8,128)(2,1)} %bitcast.114, bf16[1,2048,896]{2,1,0:T(8,128)(2,1)} %param.21), kind=kOutput, calls=%fused_computation.7 | convolution fusion | flops 2348810240 | bytes 8585216 | tf_op jit(solution)/shard_map/dot_general | solution.py:61
  66.0 4.3 %fusion.7 = f32[640,896]{1,0:T(8,128)} fusion(bf16[640,2048]{1,0:T(8,128)(2,1)S(1)} %bitcast.116, bf16[1,2048,896]{2,1,0:T(8,128)(2,1)S(1)} %copy-done.8), kind=kOutput, calls=%fused_computation.11 | convolution fusion | flops 2348810240 | bytes 8585216 | tf_op jit(solution)/shard_map/dot_general | solution.py:62
  70.4 23.2 %all-gather.8.cloned.1.call-done = bf16[4,160,2048]{2,1,0:T(8,128)(2,1)} async-done(((bf16[4,160,256]{2,1,0:T(8,128)(2,1)}), bf16[4,160,2048]{2,1,0:T(8,128)(2,1)}) %all-gather.8.cloned.1.call-update) | async-done | bytes 2621456 | tf_op jit(solution)/shard_map/all_gather | solution.py:124
  93.6 7.8 %multiply_convert_fusion.1 = (bf16[640,896]{1,0:T(8,128)(2,1)S(1)}, bf16[640,896]{1,0:T(8,128)(2,1)S(1)}) fusion(f32[640,896]{1,0:T(8,128)} %fusion.3, f32[640,896]{1,0:T(8,128)} %fusion.7, bf16[640,2048]{1,0:T(8,128)(2,1)} %bitcast.118, bf16[1,896,2048]{2,1,0:T(8,128)(2,1)} %param.23), kind=kOutput, calls=%fused_computation.20 | convolution fusion | flops 2356264960 | bytes 13172736 | tf_op jit(solution)/shard_map/dot_general | solution.py:66
  101.5 2.9 %fusion.1 = f32[640,2048]{1,0:T(8,128)S(1)} fusion(bf16[640,896]{1,0:T(8,128)(2,1)S(1)} %get-tuple-element.152, bf16[1,2048,896]{2,1,0:T(8,128)(2,1)S(1)} %copy-done.7), kind=kOutput, calls=%fused_computation.5 | convolution fusion | flops 2348810240 | bytes 10059776 | tf_op jit(solution)/shard_map/dot_general | solution.py:71
  104.4 4.2 %add_convert_fusion = bf16[640,2048]{1,0:T(8,128)(2,1)} fusion(f32[640,2048]{1,0:T(8,128)S(1)} %fusion.1, bf16[640,896]{1,0:T(8,128)(2,1)S(1)} %get-tuple-element.151, bf16[1,2048,896]{2,1,0:T(8,128)(2,1)S(1)} %copy-done.9), kind=kOutput, calls=%fused_computation.4 | convolution fusion | flops 2351431680 | bytes 12681216 | tf_op jit(solution)/shard_map/dot_general | solution.py:72
  109.5 1.0 fusion.23
  110.7 34.2 %reduce-scatter.3.cloned.1.call-done = bf16[4,160,256]{2,1,0:T(8,128)(2,1)} async-done(((bf16[4,160,2048]{2,1,0:T(8,128)(2,1)}), bf16[4,160,256]{2,1,0:T(8,128)(2,1)}) %reduce-scatter.3.cloned.1.call-update) | async-done | bytes 327696 | tf_op jit(solution)/shard_map/reduce_scatter | solution.py:133
  144.9 3.7 %all-to-all-start.2 = ((bf16[4,160,256]{2,1,0:T(8,128)(2,1)}), bf16[4,160,256]{2,1,0:T(8,128)(2,1)S(1)}, u32[]{:S(2)}, u32[]{:S(2)}) async-start(bf16[4,160,256]{2,1,0:T(8,128)(2,1)} %reduce-scatter.3.cloned.1.call-done), calls=%async_computation.3 | async-start | bytes 655360 | tf_op jit(solution)/shard_map/all_to_all | solution.py:139
  150.8 3.3 %all-to-all-done.2 = bf16[4,160,256]{2,1,0:T(8,128)(2,1)S(1)} async-done(((bf16[4,160,256]{2,1,0:T(8,128)(2,1)}), bf16[4,160,256]{2,1,0:T(8,128)(2,1)S(1)}, u32[]{:S(2)}, u32[]{:S(2)}) %all-to-all-start.2) | async-done | bytes 327712 | tf_op jit(solution)/shard_map/all_to_all | solution.py:139
  155.1 7.4 %convert_bitcast_fusion.1 = bf16[1,2048,896]{2,1,0:T(8,128)(2,1)} fusion(bf16[640,2048]{1,0:T(8,128)(2,1)} %bitcast.115, bf16[640,896]{1,0:T(8,128)(2,1)} %copy-done.18), kind=kOutput, calls=%fused_computation.16 | convolution fusion | flops 2350645248 | bytes 7438336 | tf_op jit(solution)/shard_map/dot_general | solution.py:81
  162.6 4.9 %convert_bitcast_fusion.2 = bf16[1,2048,896]{2,1,0:T(8,128)(2,1)} fusion(bf16[640,2048]{1,0:T(8,128)(2,1)S(1)} %bitcast.117, bf16[640,896]{1,0:T(8,128)(2,1)S(1)} %copy-done.15), kind=kOutput, calls=%fused_computation.17 | convolution fusion | flops 2350645248 | bytes 7438336 | tf_op jit(solution)/shard_map/dot_general | solution.py:78
  167.5 4.6 %convert_bitcast_fusion = bf16[1,896,2048]{2,1,0:T(8,128)(2,1)} fusion(bf16[640,2048]{1,0:T(8,128)(2,1)S(1)} %bitcast.119, f32[640,896]{1,0:T(8,128)S(1)} %copy-done.17, f32[640,896]{1,0:T(8,128)S(1)} %copy-done.16), kind=kOutput, calls=%fused_computation.15 | convolution fusion | flops 2354085888 | bytes 10878976 | tf_op jit(solution)/shard_map/dot_general | solution.py:84
  172.1 4.3 %all-gather.10.cloned.1.call-done = bf16[256,2048]{1,0:T(8,128)(2,1)} async-done(((bf16[256,256]{1,0:T(8,128)(2,1)}), bf16[256,2048]{1,0:T(8,128)(2,1)}) %all-gather.10.cloned.1.call-update) | async-done | bytes 1048592 | tf_op jit(solution)/shard_map/all_gather | solution.py:146
  176.4 1.7 fusion.40
  180.3 7.2 %all-gather = f32[512,1]{0,1:T(1,128)S(1)} all-gather(f32[128,1]{0,1:T(1,128)S(1)} %get-tuple-element.156), channel_id=2, replica_groups=mesh['sp'=4,'tp'=8] {'sp'}, dimensions={0}, use_global_device_ids=true | all-gather | bytes 2560 | tf_op jit(solution)/shard_map/all_gather | solution.py:15
  187.5 7.9 %all-gather.1 = f32[512,1]{0,1:T(1,128)S(1)} all-gather(f32[128,1]{0,1:T(1,128)S(1)} %get-tuple-element.155), channel_id=3, replica_groups=mesh['sp'=4,'tp'=8] {'sp'}, dimensions={0}, use_global_device_ids=true | all-gather | bytes 2560 | tf_op jit(solution)/shard_map/all_gather | solution.py:15
  195.4 1.4 convolution_convert_fusion
  201.1 19.8 %reduce-scatter.5.cloned.1.call-done = bf16[512,128]{1,0:T(8,128)(2,1)} async-done(((bf16[2048,128]{1,0:T(8,128)(2,1)}), bf16[512,128]{1,0:T(8,128)(2,1)}) %reduce-scatter.5.cloned.1.call-update) | async-done | bytes 131088 | tf_op jit(solution)/shard_map/reduce_scatter | solution.py:218
  (225 shorter events, 15.3 us)
Async XLA Ops:
  7.2 169.2 %copy-start = (bf16[128,2048]{1,0:T(8,128)(2,1)S(1)}, bf16[128,2048]{1,0:T(8,128)(2,1)}, u32[]{:S(2)}) copy-start(bf16[128,2048]{1,0:T(8,128)(2,1)} %param.24) | copy-start | bytes 1572868
  7.2 17.1 %copy-start.2 = (bf16[256,256]{1,0:T(8,128)(2,1)S(1)}, bf16[256,256]{1,0:T(8,128)(2,1)}, u32[]{:S(2)}) copy-start(bf16[256,256]{1,0:T(8,128)(2,1)} %param.17) | copy-start | bytes 393220
  7.2 17.1 %copy-start.13 = (f32[256,2]{0,1:T(2,128)S(1)}, f32[256,2]{0,1:T(2,128)}, u32[]{:S(2)}) copy-start(f32[256,2]{0,1:T(2,128)} %param.20) | copy-start | bytes 6148
  7.2 51.6 %all-gather.6.cloned.1.call-start = ((), (), s32[]{:S(2)}) async-start(), calls=%async_computation.5 | async-start | bytes 2949120 | tf_op jit(solution)/shard_map/all_gather | solution.py:123
  24.2 69.4 %all-gather.8.cloned.1.call-start = ((), (), s32[]{:S(2)}) async-start(), calls=%async_computation.6 | async-start | bytes 2949120 | tf_op jit(solution)/shard_map/all_gather | solution.py:124
  34.1 110.8 %reduce-scatter.3.cloned.1.call-start = ((), (), s32[]{:S(2)}) async-start(), calls=%async_computation.7 | async-start | bytes 2949120 | tf_op jit(solution)/shard_map/reduce_scatter | solution.py:133
  58.8 7.2 %copy-start.8 = (bf16[1,2048,896]{2,1,0:T(8,128)(2,1)S(1)}, bf16[1,2048,896]{2,1,0:T(8,128)(2,1)}, u32[]{:S(2)}) copy-start(bf16[1,2048,896]{2,1,0:T(8,128)(2,1)} %param.22) | copy-start | bytes 11010052
  58.8 7.2 %copy-start.10 = (bf16[4,160,2048]{2,1,0:T(8,128)(2,1)S(1)}, bf16[4,160,2048]{2,1,0:T(8,128)(2,1)}, u32[]{:S(2)}) copy-start(bf16[4,160,2048]{2,1,0:T(8,128)(2,1)} %all-gather.6.cloned.1.call-done) | copy-start | bytes 7864324
  93.6 7.8 %copy-start.7 = (bf16[1,2048,896]{2,1,0:T(8,128)(2,1)S(1)}, bf16[1,2048,896]{2,1,0:T(8,128)(2,1)}, u32[]{:S(2)}) copy-start(bf16[1,2048,896]{2,1,0:T(8,128)(2,1)} %param.21) | copy-start | bytes 11010052
  101.4 3.0 %copy-start.14 = (bf16[640,896]{1,0:T(8,128)(2,1)}, bf16[640,896]{1,0:T(8,128)(2,1)S(1)}, u32[]{:S(2)}) copy-start(bf16[640,896]{1,0:T(8,128)(2,1)S(1)} %get-tuple-element.152) | copy-start | bytes 3440644
  101.4 3.0 %copy-start.18 = (bf16[640,896]{1,0:T(8,128)(2,1)}, bf16[640,896]{1,0:T(8,128)(2,1)S(1)}, u32[]{:S(2)}) copy-start(bf16[640,896]{1,0:T(8,128)(2,1)S(1)} %get-tuple-element.151) | copy-start | bytes 3440644
  101.4 2.9 %copy-start.9 = (bf16[1,2048,896]{2,1,0:T(8,128)(2,1)S(1)}, bf16[1,2048,896]{2,1,0:T(8,128)(2,1)}, u32[]{:S(2)}) copy-start(bf16[1,2048,896]{2,1,0:T(8,128)(2,1)} %param.22) | copy-start | bytes 11010052
  108.6 41.1 %copy-start.5 = (bf16[128,256]{1,0:T(8,128)(2,1)S(1)}, bf16[128,256]{1,0:T(8,128)(2,1)}, u32[]{:S(2)}) copy-start(bf16[128,256]{1,0:T(8,128)(2,1)} %param.27) | copy-start | bytes 196612
  108.6 41.2 %copy-start.6 = (bf16[128,256]{1,0:T(8,128)(2,1)S(1)}, bf16[128,256]{1,0:T(8,128)(2,1)}, u32[]{:S(2)}) copy-start(bf16[128,256]{1,0:T(8,128)(2,1)} %param.26) | copy-start | bytes 196612
  108.6 41.3 %copy-start.3 = (f32[128,256]{1,0:T(8,128)S(1)}, f32[128,256]{1,0:T(8,128)}, u32[]{:S(2)}) copy-start(f32[128,256]{1,0:T(8,128)} %param.31) | copy-start | bytes 393220
  144.9 9.2 %all-to-all-start.2 = ((bf16[4,160,256]{2,1,0:T(8,128)(2,1)}), bf16[4,160,256]{2,1,0:T(8,128)(2,1)S(1)}, u32[]{:S(2)}, u32[]{:S(2)}) async-start(bf16[4,160,256]{2,1,0:T(8,128)(2,1)} %reduce-scatter.3.cloned.1.call-done), calls=%async_computation.3 | async-start | bytes 655360 | tf_op jit(solution)/shard_map/all_to_all | solution.py:139
  148.5 27.9 %all-gather.10.cloned.1.call-start = ((), (), s32[]{:S(2)}) async-start(), calls=%async_computation.8 | async-start | bytes 1179648 | tf_op jit(solution)/shard_map/all_gather | solution.py:146
  155.1 7.5 %copy-start.15 = (bf16[640,896]{1,0:T(8,128)(2,1)S(1)}, bf16[640,896]{1,0:T(8,128)(2,1)}, u32[]{:S(2)}) copy-start(bf16[640,896]{1,0:T(8,128)(2,1)} %copy-done.14) | copy-start | bytes 3440644
  155.1 65.8 %reduce-scatter.5.cloned.1.call-start = ((), (), s32[]{:S(2)}) async-start(), calls=%async_computation.9 | async-start | bytes 655360 | tf_op jit(solution)/shard_map/reduce_scatter | solution.py:218
  155.1 7.4 %copy-start.11 = (bf16[4,160,2048]{2,1,0:T(8,128)(2,1)S(1)}, bf16[4,160,2048]{2,1,0:T(8,128)(2,1)}, u32[]{:S(2)}) copy-start(bf16[4,160,2048]{2,1,0:T(8,128)(2,1)} %all-gather.6.cloned.1.call-done) | copy-start | bytes 7864324
  162.5 4.9 %copy-start.12 = (bf16[4,160,2048]{2,1,0:T(8,128)(2,1)S(1)}, bf16[4,160,2048]{2,1,0:T(8,128)(2,1)}, u32[]{:S(2)}) copy-start(bf16[4,160,2048]{2,1,0:T(8,128)(2,1)} %all-gather.8.cloned.1.call-done) | copy-start | bytes 7864324
  162.5 4.9 %copy-start.16 = (f32[640,896]{1,0:T(8,128)S(1)}, f32[640,896]{1,0:T(8,128)}, u32[]{:S(2)}) copy-start(f32[640,896]{1,0:T(8,128)} %fusion.3) | copy-start | bytes 6881284
  162.6 4.9 %copy-start.17 = (f32[640,896]{1,0:T(8,128)S(1)}, f32[640,896]{1,0:T(8,128)}, u32[]{:S(2)}) copy-start(f32[640,896]{1,0:T(8,128)} %fusion.7) | copy-start | bytes 6881284
  178.5 16.9 %copy-start.1 = (bf16[256,2048]{1,0:T(8,128)(2,1)S(1)}, bf16[256,2048]{1,0:T(8,128)(2,1)}, u32[]{:S(2)}) copy-start(bf16[256,2048]{1,0:T(8,128)(2,1)} %all-gather.10.cloned.1.call-done) | copy-start | bytes 3145732
  (1 other events, 0.8 us)
Sparse Core Ops, SparseCore 0:
  24.3 34.4 all-gather.5
  60.4 33.1 all-gather.7
  108.7 36.0 reduce-scatter.2
  155.2 21.1 all-gather.9
  196.9 23.9 reduce-scatter.4
where the time goes:
time: 230 us; the launch traced here: 229 us
  waiting for transfers between devices  110 us (48%)
  matrix products  52.8 us (23%)
  blocking collectives  36 us (16%)
  between operations  14.9 us (6%)
  local copies, waits for them, and re-layouts  7.07 us (3%)
  other arithmetic  4.91 us (2%)
  starting transfers between devices  3.85 us (2%)
    reduce_scatter x1, waiting for transfers between devices, local(): lax.psum_scatter(width_part.reshape(experts, capacity, full_width).astype...  34.2 us
    all_gather x1, waiting for transfers between devices, local(): lax.all_gather(part_rows, 'tp', axis=2, tiled=True)  24.6 us
    all_gather x1, waiting for transfers between devices, local(): lax.all_gather(portion_adjoint, 'tp', axis=2, tiled=True)  23.2 us
    reduce_scatter x1, waiting for transfers between devices, local(): lax.psum_scatter(lax.dot_general(full_grad, mixed, (((0,), (1,)), ((), ()...  19.8 us
    all_gather x2, blocking collectives, prefix(): pieces = jax.tree.map(lambda part: lax.all_gather(part, axis), value)  15 us
    all_to_all x1, blocking collectives, local(): lax.all_to_all(sent_rows.reshape(experts, capacity, -1), 'sp', split_axis...  11.7 us
    all_to_all x1, blocking collectives, local(): lax.all_to_all(sent_cot.reshape(experts, capacity, -1), 'sp', split_axis=...  9.32 us
    dot_general x1, matrix products, expert_work(): lax.dot_general(slot_cot, w_down, minor, preferred_element_type=jnp.float32)  7.79 us
  transfers between devices with their start and end apart: 6, of which 6 were waited for; matrix products, arithmetic and copies ran while one was open for 16% of the time, Pallas kernels for 0%

commit v1 on v0

--- a/solution.py
+++ b/solution.py
@@ -1,6 +1,10 @@
+import functools
+
 import jax
 import jax.numpy as jnp
 from jax import lax
+from jax.experimental import pallas as pl
+from jax.experimental.pallas import tpu as pltpu
 from jax.sharding import PartitionSpec as P
 
 HEAD_DIM = 64
@@ -10,28 +14,8 @@
 RATE_SCALE = 8.0
 
 
-def prefix(value, axis, join, neutral):
-    count, mine = (lax.axis_size(axis), lax.axis_index(axis))
-    pieces = jax.tree.map(lambda part: lax.all_gather(part, axis), value)
-    pieces = jax.tree.map(lambda part: part[::-1], pieces)
-    mine = count - 1 - mine
-    so_far = jax.tree.map(
-        lambda part, zero: jnp.full_like(part, 0) + jnp.asarray(zero, part.dtype), value, neutral
-    )
-
-    def turn(position, so_far):
-        longer = join(so_far, jax.tree.map(lambda part: part[position], pieces))
-        return jax.tree.map(lambda new, old: jnp.where(position < mine, new, old), longer, so_far)
-
-    return lax.fori_loop(0, count - 1, turn, so_far)
-
-
 def link_pairs(left_pair, right_pair):
     return (left_pair[0] * right_pair[0], right_pair[0] * left_pair[1] + right_pair[1])
-
-
-def later_first(earlier_pair, later_pair):
-    return (earlier_pair[0] * later_pair[0], later_pair[1] + later_pair[0] * earlier_pair[1])
 
 
 def routing_tables(routes, experts, capacity):
@@ -45,15 +29,301 @@
     return jnp.transpose(target)[:, None, :] == slot_ids[None, :, None]
 
 
-def spread(placing, route_hits, rows_in, cot_in, route_weights):
-    sent_rows = jnp.dot(placing, rows_in, preferred_element_type=jnp.float32).astype(jnp.bfloat16)
-    scaled = (
-        jnp.transpose(route_weights)[:, :, None] * cot_in.astype(jnp.float32)[None, :, :]
-    ).astype(jnp.bfloat16)
-    sent_cot = jnp.einsum(
-        "kst,ktd->sd", route_hits, scaled, preferred_element_type=jnp.float32
-    ).astype(jnp.bfloat16)
-    return (sent_rows, sent_cot)
+CORES = 2
+VMEM = pl.BlockSpec(memory_space=pltpu.VMEM)
+
+
+def across(place, step, size):
+    result, bit = 0, 1
+    while bit < size:
+        result = result + lax.rem(lax.div(place, bit) + (step // bit) % 2, 2) * bit
+        bit *= 2
+    return result
+
+
+def send(source, target, sems, index, device):
+    return pltpu.make_async_remote_copy(
+        src_ref=source,
+        dst_ref=target,
+        send_sem=sems[0].at[index],
+        recv_sem=sems[1].at[index],
+        device_id=device,
+        device_id_type=pl.DeviceIdType.MESH,
+    )
+
+
+def greet(devices):
+    barrier = pltpu.get_barrier_semaphore()
+    for device in devices:
+        pl.semaphore_signal(
+            barrier, inc=1, device_id=device, device_id_type=pl.DeviceIdType.MESH
+        )
+    pl.semaphore_wait(barrier, len(devices))
+
+
+def position(deep):
+    sp, tp = lax.axis_index("sp"), lax.axis_index("tp")
+    z, core = lax.div(tp, CORES), lax.rem(tp, CORES)
+    return sp, tp, z, core, (sp, z * CORES + 1 - core)
+
+
+def columns(block, width):
+    return pl.ds(pl.multiple_of(block * width, width), width)
+
+
+def dispatch_kernel(
+    experts,
+    deep,
+    rows_in,
+    cot_in,
+    placing,
+    slot_weight,
+    rows_out,
+    cot_out,
+    held,
+    stage,
+    z_send,
+    z_recv,
+    p_send,
+    p_recv,
+    c_send,
+    c_recv,
+):
+    sp, tp, z, core, partner = position(deep)
+    width = rows_in.shape[1]
+    planes = [(across(sp, k, experts), tp) for k in range(experts)]
+    levels = [across(z, d, deep) for d in range(deep)]
+    lines = [(sp, level * CORES + core) for level in levels]
+    greet(planes[1:] + lines[1:] + [partner])
+    sources, outs = (rows_in, cot_in), (rows_out, cot_out)
+    line_copies, plane_copies = {}, {}
+    for a in range(2):
+        for d in range(1, deep):
+            copy = send(sources[a], held.at[a, d - 1], (z_send, z_recv), (a, d), lines[d])
+            copy.start()
+            line_copies[a, d] = copy
+    for a in range(2):
+        for d in range(deep):
+            if d:
+                line_copies[a, d].wait_recv()
+            block = held[a, d - 1] if d else sources[a][...]
+            here = columns(levels[d] * CORES + core, width)
+            for k in list(range(1, experts)) + [0]:
+                expert = planes[k][0]
+                piece = jnp.dot(placing[expert], block, preferred_element_type=jnp.float32)
+                if a:
+                    piece = piece * slot_weight[expert]
+                piece = piece.astype(jnp.bfloat16)
+                if k == 0:
+                    outs[a][sp, :, here] = piece
+                else:
+                    stage[a, d, k - 1] = piece
+                    copy = send(
+                        stage.at[a, d, k - 1],
+                        outs[a].at[sp, :, here],
+                        (p_send, p_recv),
+                        (a, d, k),
+                        planes[k],
+                    )
+                    copy.start()
+                    plane_copies[a, d, k] = copy
+    core_copies = []
+    for a in range(2):
+        for d in range(deep):
+            for k in range(1, experts):
+                plane_copies[a, d, k].wait_recv()
+            here = columns(levels[d] * CORES + core, width)
+            copy = send(
+                outs[a].at[:, :, here], outs[a].at[:, :, here], (c_send, c_recv), (a, d), partner
+            )
+            copy.start()
+            core_copies.append(copy)
+    for copy in core_copies:
+        copy.wait_recv()
+    for copy in core_copies + list(plane_copies.values()) + list(line_copies.values()):
+        copy.wait_send()
+
+
+def dispatch(rows_in, cot_in, placing, slot_weight):
+    experts, capacity, tok_rows = placing.shape
+    deep = lax.axis_size("tp") // CORES
+    width = rows_in.shape[1]
+    out = jax.ShapeDtypeStruct((experts, capacity, width * deep * CORES), jnp.bfloat16)
+    sems = [(2, deep), (2, deep, experts), (2, deep)]
+    return pl.pallas_call(
+        functools.partial(dispatch_kernel, experts, deep),
+        out_shape=(out, out),
+        in_specs=[VMEM] * 4,
+        out_specs=(VMEM, VMEM),
+        scratch_shapes=[
+            pltpu.VMEM((2, deep - 1, tok_rows, width), jnp.bfloat16),
+            pltpu.VMEM((2, deep, experts - 1, capacity, width), jnp.bfloat16),
+        ]
+        + [pltpu.SemaphoreType.DMA(shape) for shape in sems for _ in range(2)],
+        compiler_params=pltpu.CompilerParams(
+            collective_id=0, has_side_effects=True, vmem_limit_bytes=48 << 20
+        ),
+    )(rows_in, cot_in, placing, slot_weight)
+
+
+def combine_kernel(
+    experts,
+    deep,
+    parts,
+    cot_in,
+    taking,
+    full_out,
+    paired,
+    stage,
+    plane,
+    line_out,
+    line_in,
+    c_send,
+    c_recv,
+    p_send,
+    p_recv,
+    z_send,
+    z_recv,
+    g_send,
+    g_recv,
+    f_send,
+    f_recv,
+):
+    sp, tp, z, core, partner = position(deep)
+    width = cot_in.shape[1]
+    planes = [(across(sp, k, experts), tp) for k in range(experts)]
+    levels = [across(z, d, deep) for d in range(deep)]
+    lines = [(sp, level * CORES + core) for level in levels]
+    greet(planes[1:] + lines[1:] + [partner])
+    order = list(range(deep - 1, -1, -1))
+    started, core_copies, plane_copies, line_copies = [], {}, {}, {}
+    for d in order:
+        theirs = columns(levels[d] * CORES + 1 - core, width)
+        copy = send(parts.at[:, :, theirs], paired.at[d], (c_send, c_recv), d, partner)
+        copy.start()
+        core_copies[d] = copy
+        started.append(copy)
+    for d in order:
+        core_copies[d].wait_recv()
+        here = columns(levels[d] * CORES + core, width)
+        for k in list(range(1, experts)) + [0]:
+            home = planes[k][0]
+            piece = (
+                parts[home, :, here].astype(jnp.float32) + paired[d, home].astype(jnp.float32)
+            ).astype(jnp.bfloat16)
+            if k == 0:
+                plane[d, 0] = piece
+            else:
+                stage[d, k - 1] = piece
+                copy = send(
+                    stage.at[d, k - 1], plane.at[d, k], (p_send, p_recv), (d, k), planes[k]
+                )
+                copy.start()
+                plane_copies[d, k] = copy
+                started.append(copy)
+    total = cot_in[...].astype(jnp.float32)
+    for d in order:
+        summed = jnp.dot(taking[sp], plane[d, 0], preferred_element_type=jnp.float32)
+        for k in range(1, experts):
+            plane_copies[d, k].wait_recv()
+            summed = summed + jnp.dot(
+                taking[planes[k][0]], plane[d, k], preferred_element_type=jnp.float32
+            )
+        if d == 0:
+            total = total + summed
+        else:
+            line_out[d - 1] = summed.astype(jnp.bfloat16)
+            copy = send(line_out.at[d - 1], line_in.at[d - 1], (z_send, z_recv), d, lines[d])
+            copy.start()
+            line_copies[d] = copy
+            started.append(copy)
+    for d in order[:-1]:
+        line_copies[d].wait_recv()
+        total = total + line_in[d - 1].astype(jnp.float32)
+    mine = columns(tp, width)
+    full_out[:, mine] = total.astype(jnp.bfloat16)
+    gathers, forwards = {}, []
+    for d in range(1, deep):
+        copy = send(full_out.at[:, mine], full_out.at[:, mine], (g_send, g_recv), d, lines[d])
+        copy.start()
+        gathers[d] = copy
+        started.append(copy)
+    for d in range(deep):
+        if d:
+            gathers[d].wait_recv()
+        here = columns(levels[d] * CORES + core, width)
+        copy = send(full_out.at[:, here], full_out.at[:, here], (f_send, f_recv), d, partner)
+        copy.start()
+        forwards.append(copy)
+    for copy in forwards:
+        copy.wait_recv()
+    for copy in started + forwards:
+        copy.wait_send()
+
+
+def combine(parts, cot_in, taking):
+    experts, capacity, full_width = parts.shape
+    tok_rows, width = cot_in.shape
+    deep = lax.axis_size("tp") // CORES
+    sems = [(deep,), (deep, experts), (deep,), (deep,), (deep,)]
+    return pl.pallas_call(
+        functools.partial(combine_kernel, experts, deep),
+        out_shape=jax.ShapeDtypeStruct((tok_rows, full_width), jnp.bfloat16),
+        in_specs=[VMEM] * 3,
+        out_specs=VMEM,
+        scratch_shapes=[
+            pltpu.VMEM((deep, experts, capacity, width), jnp.bfloat16),
+            pltpu.VMEM((deep, experts - 1, capacity, width), jnp.bfloat16),
+            pltpu.VMEM((deep, experts, capacity, width), jnp.bfloat16),
+            pltpu.VMEM((deep - 1, tok_rows, width), jnp.bfloat16),
+            pltpu.VMEM((deep - 1, tok_rows, width), jnp.bfloat16),
+        ]
+        + [pltpu.SemaphoreType.DMA(shape) for shape in sems for _ in range(2)],
+        compiler_params=pltpu.CompilerParams(
+            collective_id=1, has_side_effects=True, vmem_limit_bytes=48 << 20
+        ),
+    )(parts, cot_in, taking)
+
+
+def closing_kernel(
+    count, summary, product, summaries, products, s_send, s_recv, p_send, p_recv
+):
+    sp, tp = lax.axis_index("sp"), lax.axis_index("tp")
+    width = products.shape[2]
+    peers = [(across(sp, k, count), tp) for k in range(count)]
+    greet(peers[1:])
+    copies = []
+    for k in range(1, count):
+        copies.append(send(summary, summaries.at[sp], (s_send, s_recv), k, peers[k]))
+        copies[-1].start()
+    for k in range(1, count):
+        theirs = columns(peers[k][0], width)
+        copies.append(
+            send(product.at[:, theirs], products.at[k], (p_send, p_recv), k, peers[k])
+        )
+        copies[-1].start()
+    summaries[sp] = summary[...]
+    products[0] = product[:, columns(sp, width)]
+    for copy in copies:
+        copy.wait()
+
+
+def closing(summary, product):
+    count = lax.axis_size("sp")
+    channels, full_width = product.shape
+    return pl.pallas_call(
+        functools.partial(closing_kernel, count),
+        out_shape=(
+            jax.ShapeDtypeStruct((count,) + summary.shape, summary.dtype),
+            jax.ShapeDtypeStruct((count, channels, full_width // count), product.dtype),
+        ),
+        in_specs=[VMEM] * 2,
+        out_specs=(VMEM, VMEM),
+        scratch_shapes=[pltpu.SemaphoreType.DMA((count,)) for _ in range(4)],
+        compiler_params=pltpu.CompilerParams(
+            collective_id=2, has_side_effects=True, vmem_limit_bytes=16 << 20
+        ),
+    )(summary, product)
 
 
 def expert_work(slot_rows, slot_cot, w_gate, w_up, w_down):
@@ -108,21 +378,13 @@
     tok_rows = cotangent.shape[0]
     capacity = 5 * tok_rows * TOP_K // (4 * experts)
     route_hits = routing_tables(routes, experts, capacity)
-    placing = jnp.sum(route_hits.astype(jnp.int32), axis=0).astype(jnp.bfloat16)
-    hit_table = route_hits.astype(jnp.bfloat16)
-    sent_rows, sent_cot = spread(placing, hit_table, block_input, cotangent, route_weights)
-    part_rows, portion_adjoint = (
-        lax.all_to_all(
-            sent_rows.reshape(experts, capacity, -1), "sp", split_axis=0, concat_axis=0, tiled=True
-        ),
-        lax.all_to_all(
-            sent_cot.reshape(experts, capacity, -1), "sp", split_axis=0, concat_axis=0, tiled=True
-        ),
-    )
-    got_rows, got_cot = (
-        lax.all_gather(part_rows, "tp", axis=2, tiled=True),
-        lax.all_gather(portion_adjoint, "tp", axis=2, tiled=True),
-    )
+    hits = jnp.sum(route_hits.astype(jnp.float32), axis=0)
+    placing = hits.astype(jnp.bfloat16).reshape(experts, capacity, tok_rows)
+    taking = jnp.swapaxes(placing, 1, 2)
+    slot_weight = jnp.sum(
+        jnp.where(route_hits, jnp.transpose(route_weights)[:, None, :], 0.0), axis=(0, 2)
+    ).reshape(experts, capacity, 1)
+    got_rows, got_cot = dispatch(block_input, cotangent, placing, slot_weight)
     full_width = got_rows.shape[2]
     slot_rows = got_rows.reshape(-1, full_width)
     slot_cot = got_cot.reshape(-1, full_width)
@@ -130,20 +392,9 @@
         slot_rows, slot_cot, gate_weight[0], up_weight[0], down_weight[0]
     )
     gate_grad, up_grad, down_grad = weight_grads(slot_rows, slot_cot, hidden, d_gate, d_up)
-    summed = lax.psum_scatter(
-        width_part.reshape(experts, capacity, full_width).astype(jnp.bfloat16),
-        "tp",
-        scatter_dimension=2,
-        tiled=True,
-    )
-    handed_result = lax.all_to_all(summed, "sp", split_axis=0, concat_axis=0, tiled=True).reshape(
-        experts * capacity, -1
-    )
-    moe_grad = lax.dot_general(
-        placing, handed_result, (((0,), (0,)), ((), ())), preferred_element_type=jnp.float32
-    )
-    block_grad = (cotangent.astype(jnp.float32) + moe_grad).astype(jnp.bfloat16)
-    full_grad = lax.all_gather(block_grad, "tp", axis=1, tiled=True)
+    full_grad = combine(
+        width_part.astype(jnp.bfloat16).reshape(experts, capacity, full_width), cotangent, taking
+    )
     channels = conv_out.shape[0]
     length = conv_out.shape[1]
     head_count = channels // HEAD_DIM
@@ -182,13 +433,14 @@
     flipped = lax.associative_scan(link_pairs, (jnp.flip(shifted, 1), jnp.flip(d_state, 1)), axis=1)
     decay_prod = jnp.flip(flipped[0], 1)
     local_sum = jnp.flip(flipped[1], 1)
-    summary = (decay_val[:, 0] * decay_prod[:, 0], decay_val[:, 0] * local_sum[:, 0])
-    carried = prefix(
-        summary,
-        "sp",
-        later_first,
-        (jnp.ones((channels,), jnp.float32), jnp.zeros((channels,), jnp.float32)),
-    )[1]
+    summary = jnp.stack([decay_val[:, 0] * decay_prod[:, 0], decay_val[:, 0] * local_sum[:, 0]])
+    product = jnp.dot(mixed, full_grad, preferred_element_type=jnp.float32).astype(jnp.bfloat16)
+    summaries, products = closing(summary, product)
+    carried = jnp.zeros((channels,), jnp.float32)
+    for later in range(experts - 1, 0, -1):
+        longer = summaries[later, 1] + summaries[later, 0] * carried
+        carried = jnp.where(later > lax.axis_index("sp"), longer, carried)
+    out_weight_grad = jnp.sum(products.astype(jnp.float32), axis=0)
     state_grad = local_sum + decay_prod * carried[:, None]
     grad_log = (
         state_grad * prior_vals * decay_val
@@ -215,15 +467,6 @@
     conv_grad = (state_grad * norm_scale * input_gate + back_recur + back_input).astype(
         jnp.bfloat16
     )
-    projected = lax.psum_scatter(
-        lax.dot_general(
-            full_grad, mixed, (((0,), (1,)), ((), ())), preferred_element_type=jnp.float32
-        ).astype(jnp.bfloat16),
-        "sp",
-        scatter_dimension=0,
-        tiled=True,
-    ).astype(jnp.float32)
-    out_weight_grad = jnp.transpose(projected)
     return (gate_grad, up_grad, down_grad, out_weight_grad, conv_grad, valve_logit_derivative)
 
 

time: 230 us -> 148 us (0.64)
  waiting for transfers between devices: 110 us -> 0 us
  Pallas kernels: 0 us -> 88.4 us
  blocking collectives: 36 us -> 0 us
  between operations: 14.9 us -> 1.83 us
  matrix products: 52.8 us -> 42.2 us
  starting transfers between devices: 3.85 us -> 0 us
  local copies, waits for them, and re-layouts: 7.07 us -> 9.39 us
    pallas_call x0 -> x3, Pallas kernels: none -> 88.4 us  [the longest x1 41.8 us: dispatch(): pl.pallas_call(functools.partial(dispatch_kernel, experts, deep), out_sha...]
    reduce_scatter x2 -> x0, waiting for transfers between devices: 54 us -> none  [the longest x1 34.2 us: local(): lax.psum_scatter(width_part.reshape(experts, capacity, full_width).astype...]
    all_gather x3 -> x0, waiting for transfers between devices: 52.2 us -> none  [the longest x1 24.6 us: local(): lax.all_gather(part_rows, 'tp', axis=2, tiled=True)]
    all_to_all x2 -> x0, blocking collectives: 21 us -> none  [the longest x1 11.7 us: local(): lax.all_to_all(sent_rows.reshape(experts, capacity, -1), 'sp', split_axis...]
    all_gather x2 -> x0, blocking collectives: 15 us -> none  [prefix(): pieces = jax.tree.map(lambda part: lax.all_gather(part, axis), value)]
    dot_general x1, matrix products: 7.79 us -> 3.56 us  [expert_work(): lax.dot_general(slot_cot, w_down, minor, preferred_element_type=jnp.float32)]
    all_to_all x1 -> x0, starting transfers between devices: 3.66 us -> none  [local(): lax.all_to_all(summed, 'sp', split_axis=0, concat_axis=0, tiled=True)]
    dot_general x4 -> x1, matrix products: 3.98 us -> 0.48 us  [local(): jnp.dot(mixed, full_grad, preferred_element_type=jnp.float32)]
  transfers between devices with their start and end apart: 6 -> 0, of which waited for: 6 -> 0; matrix products, arithmetic and copies ran while one was open for 16% -> 0% of each run, Pallas kernels for 0% -> 0%
where the time goes in v1:
time: 148 us; the launch traced here: 147 us
  Pallas kernels  88.4 us (60%)
  matrix products  42.2 us (29%)
  local copies, waits for them, and re-layouts  9.39 us (6%)
  other arithmetic  5.45 us (4%)
  between operations  1.83 us (1%)
    pallas_call x1, Pallas kernels, dispatch(): pl.pallas_call(functools.partial(dispatch_kernel, experts, deep), out_sha...  41.8 us
    pallas_call x1, Pallas kernels, combine(): pl.pallas_call(functools.partial(combine_kernel, experts, deep), out_shap...  34.8 us
    pallas_call x1, Pallas kernels, closing(): pl.pallas_call(functools.partial(closing_kernel, count), out_shape=(jax.S...  11.8 us
    dot_general x1, matrix products, weight_grads(): lax.dot_general(slot_rows, d_up, major, preferred_element_type=jnp.float32)  7.39 us
    dot_general x1, matrix products, expert_work(): gate_act = jnp.dot(slot_rows, w_gate, preferred_element_type=jnp.float32)  6.84 us
    unnamed x53, local copies, waits for them, and re-layouts  6.42 us
    dot_general x1, matrix products, weight_grads(): lax.dot_general(slot_rows, d_gate, major, preferred_element_type=jnp.floa...  4.85 us
    dot_general x1, matrix products, weight_grads(): lax.dot_general(hidden, slot_cot, major, preferred_element_type=jnp.float32)  4.6 us

profile of v1, /device:TPU:0, one launch (start us, length us, event | category | flops | bytes accessed | tf_op | source)
XLA Modules:
  0.0 147.3 jit_solution(15967401074842942888)
XLA Ops:
  0.6 0.9 copy.102
  1.7 1.2 reduce-window.6
  4.5 1.0 select_reduce_fusion
  5.7 0.9 copy-done.2
  6.6 0.9 copy-done.4
  7.5 41.8 %shard_map.190 = (bf16[4,160,2048]{2,1,0:T(8,128)(2,1)S(1)}, bf16[4,160,2048]{2,1,0:T(8,128)(2,1)S(1)}) custom-call(bf16[256,256]{1,0:T(8,128)(2,1)S(1)} %copy-done.4, bf16[256,256]{1,0:T(8,128)(2,1)S(1)} %copy-done.2, bf16[4,160,256]{2,1,0:T(8,128)(2,1)S(1)} %bitcast.106, f32[4,160,1]{2,1,0:T(8,128)S(1)} %reshape.173.slot_weight), custom_call_target="tpu_custom_call" | custom-call | tf_op jit(solution)/shard_map/pallas_call | solution.py:153
  49.4 6.8 %fusion.2 = f32[640,896]{1,0:T(8,128)S(1)} fusion(bf16[640,2048]{1,0:T(8,128)(2,1)S(1)} %bitcast.112, bf16[1,2048,896]{2,1,0:T(8,128)(2,1)} %param.19), kind=kOutput, calls=%fused_computation.3 | convolution fusion | flops 2348810240 | bytes 8585216 | tf_op jit(solution)/shard_map/dot_general | solution.py:331
  56.3 2.9 %fusion.6 = f32[640,896]{1,0:T(8,128)S(1)} fusion(bf16[640,2048]{1,0:T(8,128)(2,1)S(1)} %bitcast.113, bf16[1,2048,896]{2,1,0:T(8,128)(2,1)S(1)} %copy-done.15), kind=kOutput, calls=%fused_computation.7 | convolution fusion | flops 2348810240 | bytes 8585216 | tf_op jit(solution)/shard_map/dot_general | solution.py:332
  59.2 3.6 %multiply_convert_fusion.1 = (bf16[640,896]{1,0:T(8,128)(2,1)S(1)}, bf16[640,896]{1,0:T(8,128)(2,1)S(1)}) fusion(f32[640,896]{1,0:T(8,128)S(1)} %fusion.2, f32[640,896]{1,0:T(8,128)S(1)} %fusion.6, bf16[640,2048]{1,0:T(8,128)(2,1)S(1)} %bitcast.110, bf16[1,896,2048]{2,1,0:T(8,128)(2,1)S(1)} %copy-done.13), kind=kOutput, calls=%fused_computation.16 | convolution fusion | flops 2356264960 | bytes 13172736 | tf_op jit(solution)/shard_map/dot_general | solution.py:336
  62.8 2.9 %fusion = f32[640,2048]{1,0:T(8,128)S(1)} fusion(bf16[640,896]{1,0:T(8,128)(2,1)S(1)} %get-tuple-element.45, bf16[1,2048,896]{2,1,0:T(8,128)(2,1)S(1)} %copy-done.14), kind=kOutput, calls=%fused_computation.1 | convolution fusion | flops 2348810240 | bytes 10059776 | tf_op jit(solution)/shard_map/dot_general | solution.py:341
  65.8 4.4 %add_convert_fusion = bf16[640,2048]{1,0:T(8,128)(2,1)} fusion(f32[640,2048]{1,0:T(8,128)S(1)} %fusion, bf16[640,896]{1,0:T(8,128)(2,1)S(1)} %get-tuple-element.44, bf16[1,2048,896]{2,1,0:T(8,128)(2,1)S(1)} %copy-done.15), kind=kOutput, calls=%fused_computation | convolution fusion | flops 2351431680 | bytes 12681216 | tf_op jit(solution)/shard_map/dot_general | solution.py:342
  70.4 1.7 %copy-done.1 = bf16[640,2048]{1,0:T(8,128)(2,1)S(1)} copy-done((bf16[640,2048]{1,0:T(8,128)(2,1)S(1)}, bf16[640,2048]{1,0:T(8,128)(2,1)}, u32[]{:S(2)}) %copy-start.1) | copy-done | bytes 2621464
  72.1 34.8 %shard_map.191 = bf16[256,2048]{1,0:T(8,128)(2,1)S(1)} custom-call(bf16[4,160,2048]{2,1,0:T(8,128)(2,1)S(1)} %bitcast.108, bf16[256,256]{1,0:T(8,128)(2,1)S(1)} %copy-done.3, bf16[4,256,160]{2,1,0:T(8,128)(2,1)S(1)} %bitcast.109), custom_call_target="tpu_custom_call" | custom-call | tf_op jit(solution)/shard_map/pallas_call | solution.py:269
  107.0 1.0 fusion.18
  108.1 1.0 fusion.16
  109.2 0.8 fusion.61
  113.8 11.8 %shard_map.192 = (f32[4,2,128]{2,1,0:T(2,128)S(1)}, bf16[4,128,512]{2,1,0:T(8,128)(2,1)S(1)}) custom-call(f32[2,128]{1,0:T(2,128)S(1)} %pad_maximum_fusion.13.summary, bf16[128,2048]{1,0:T(8,128)(2,1)S(1)} %convolution_convert_fusion.product), custom_call_target="tpu_custom_call" | custom-call | tf_op jit(solution)/shard_map/pallas_call | solution.py:314
  126.0 0.9 fusion.52
  127.1 0.9 fusion.49
  128.1 0.7 copy.127
  128.9 0.8 convert_reduce_fusion.1
  130.4 7.4 %convert_bitcast_fusion.1 = bf16[1,2048,896]{2,1,0:T(8,128)(2,1)} fusion(bf16[640,2048]{1,0:T(8,128)(2,1)} %bitcast.114, bf16[640,896]{1,0:T(8,128)(2,1)} %copy-done.22), kind=kOutput, calls=%fused_computation.12 | convolution fusion | flops 2350645248 | bytes 7438336 | tf_op jit(solution)/shard_map/dot_general | solution.py:351
  137.8 4.9 %convert_bitcast_fusion.2 = bf16[1,2048,896]{2,1,0:T(8,128)(2,1)} fusion(bf16[640,2048]{1,0:T(8,128)(2,1)S(1)} %bitcast.115, bf16[640,896]{1,0:T(8,128)(2,1)S(1)} %copy-done.17), kind=kOutput, calls=%fused_computation.13 | convolution fusion | flops 2350645248 | bytes 7438336 | tf_op jit(solution)/shard_map/dot_general | solution.py:348
  142.7 4.6 %convert_bitcast_fusion = bf16[1,896,2048]{2,1,0:T(8,128)(2,1)} fusion(bf16[640,2048]{1,0:T(8,128)(2,1)S(1)} %bitcast.111, f32[640,896]{1,0:T(8,128)S(1)} %copy-done.21, f32[640,896]{1,0:T(8,128)S(1)} %copy-done.19), kind=kOutput, calls=%fused_computation.11 | convolution fusion | flops 2354085888 | bytes 10878976 | tf_op jit(solution)/shard_map/dot_general | solution.py:354
  (207 shorter events, 6.9 us)
Async XLA Ops:
  0.6 109.8 %copy-start = (bf16[128,2048]{1,0:T(8,128)(2,1)S(1)}, bf16[128,2048]{1,0:T(8,128)(2,1)}, u32[]{:S(2)}) copy-start(bf16[128,2048]{1,0:T(8,128)(2,1)} %param.22) | copy-start | bytes 1572868
  5.7 0.9 copy-start.2
  6.6 0.9 copy-start.4
  49.4 6.9 %copy-start.7 = (bf16[4,160,2048]{2,1,0:T(8,128)(2,1)}, bf16[4,160,2048]{2,1,0:T(8,128)(2,1)S(1)}, u32[]{:S(2)}) copy-start(bf16[4,160,2048]{2,1,0:T(8,128)(2,1)S(1)} %get-tuple-element.10) | copy-start | bytes 7864324
  49.4 9.8 %copy-start.5 = (bf16[4,160,2048]{2,1,0:T(8,128)(2,1)}, bf16[4,160,2048]{2,1,0:T(8,128)(2,1)S(1)}, u32[]{:S(2)}) copy-start(bf16[4,160,2048]{2,1,0:T(8,128)(2,1)S(1)} %get-tuple-element.11) | copy-start | bytes 7864324
  49.4 6.9 %copy-start.15 = (bf16[1,2048,896]{2,1,0:T(8,128)(2,1)S(1)}, bf16[1,2048,896]{2,1,0:T(8,128)(2,1)}, u32[]{:S(2)}) copy-start(bf16[1,2048,896]{2,1,0:T(8,128)(2,1)} %param.20) | copy-start | bytes 11010052
  56.3 2.9 %copy-start.18 = (f32[640,896]{1,0:T(8,128)}, f32[640,896]{1,0:T(8,128)S(1)}, u32[]{:S(2)}) copy-start(f32[640,896]{1,0:T(8,128)S(1)} %fusion.2) | copy-start | bytes 6881284
  56.3 2.9 %copy-start.13 = (bf16[1,896,2048]{2,1,0:T(8,128)(2,1)S(1)}, bf16[1,896,2048]{2,1,0:T(8,128)(2,1)}, u32[]{:S(2)}) copy-start(bf16[1,896,2048]{2,1,0:T(8,128)(2,1)} %param.21) | copy-start | bytes 11010052
  59.2 3.6 %copy-start.20 = (f32[640,896]{1,0:T(8,128)}, f32[640,896]{1,0:T(8,128)S(1)}, u32[]{:S(2)}) copy-start(f32[640,896]{1,0:T(8,128)S(1)} %fusion.6) | copy-start | bytes 6881284
  59.2 3.6 %copy-start.14 = (bf16[1,2048,896]{2,1,0:T(8,128)(2,1)S(1)}, bf16[1,2048,896]{2,1,0:T(8,128)(2,1)}, u32[]{:S(2)}) copy-start(bf16[1,2048,896]{2,1,0:T(8,128)(2,1)} %param.19) | copy-start | bytes 11010052
  62.8 2.9 %copy-start.16 = (bf16[640,896]{1,0:T(8,128)(2,1)}, bf16[640,896]{1,0:T(8,128)(2,1)S(1)}, u32[]{:S(2)}) copy-start(bf16[640,896]{1,0:T(8,128)(2,1)S(1)} %get-tuple-element.45) | copy-start | bytes 3440644
  62.8 2.9 %copy-start.22 = (bf16[640,896]{1,0:T(8,128)(2,1)}, bf16[640,896]{1,0:T(8,128)(2,1)S(1)}, u32[]{:S(2)}) copy-start(bf16[640,896]{1,0:T(8,128)(2,1)S(1)} %get-tuple-element.44) | copy-start | bytes 3440644
  65.8 4.6 %copy-start.3 = (bf16[256,256]{1,0:T(8,128)(2,1)S(1)}, bf16[256,256]{1,0:T(8,128)(2,1)}, u32[]{:S(2)}) copy-start(bf16[256,256]{1,0:T(8,128)(2,1)} %cot_in.3) | copy-start | bytes 393220
  70.4 1.7 %copy-start.1 = (bf16[640,2048]{1,0:T(8,128)(2,1)S(1)}, bf16[640,2048]{1,0:T(8,128)(2,1)}, u32[]{:S(2)}) copy-start(bf16[640,2048]{1,0:T(8,128)(2,1)} %add_convert_fusion) | copy-start | bytes 7864324
  72.1 34.9 %copy-start.11 = (bf16[128,256]{1,0:T(8,128)(2,1)S(1)}, bf16[128,256]{1,0:T(8,128)(2,1)}, u32[]{:S(2)}) copy-start(bf16[128,256]{1,0:T(8,128)(2,1)} %param.23) | copy-start | bytes 196612
  72.1 37.8 %copy-start.10 = (bf16[128,256]{1,0:T(8,128)(2,1)S(1)}, bf16[128,256]{1,0:T(8,128)(2,1)}, u32[]{:S(2)}) copy-start(bf16[128,256]{1,0:T(8,128)(2,1)} %param.25) | copy-start | bytes 196612
  72.1 38.1 %copy-start.12 = (bf16[128,256]{1,0:T(8,128)(2,1)S(1)}, bf16[128,256]{1,0:T(8,128)(2,1)}, u32[]{:S(2)}) copy-start(bf16[128,256]{1,0:T(8,128)(2,1)} %param.24) | copy-start | bytes 196612
  72.1 38.2 %copy-start.9 = (f32[128,256]{1,0:T(8,128)S(1)}, f32[128,256]{1,0:T(8,128)}, u32[]{:S(2)}) copy-start(f32[128,256]{1,0:T(8,128)} %param.29) | copy-start | bytes 393220
  130.4 7.4 %copy-start.8 = (bf16[4,160,2048]{2,1,0:T(8,128)(2,1)S(1)}, bf16[4,160,2048]{2,1,0:T(8,128)(2,1)}, u32[]{:S(2)}) copy-start(bf16[4,160,2048]{2,1,0:T(8,128)(2,1)} %copy-done.7) | copy-start | bytes 7864324
  130.4 7.4 %copy-start.17 = (bf16[640,896]{1,0:T(8,128)(2,1)S(1)}, bf16[640,896]{1,0:T(8,128)(2,1)}, u32[]{:S(2)}) copy-start(bf16[640,896]{1,0:T(8,128)(2,1)} %copy-done.16) | copy-start | bytes 3440644
  137.8 4.9 %copy-start.6 = (bf16[4,160,2048]{2,1,0:T(8,128)(2,1)S(1)}, bf16[4,160,2048]{2,1,0:T(8,128)(2,1)}, u32[]{:S(2)}) copy-start(bf16[4,160,2048]{2,1,0:T(8,128)(2,1)} %copy-done.5) | copy-start | bytes 7864324
  137.8 4.9 %copy-start.19 = (f32[640,896]{1,0:T(8,128)S(1)}, f32[640,896]{1,0:T(8,128)}, u32[]{:S(2)}) copy-start(f32[640,896]{1,0:T(8,128)} %copy-done.18) | copy-start | bytes 6881284
  137.8 4.9 %copy-start.21 = (f32[640,896]{1,0:T(8,128)S(1)}, f32[640,896]{1,0:T(8,128)}, u32[]{:S(2)}) copy-start(f32[640,896]{1,0:T(8,128)} %copy-done.20) | copy-start | bytes 6881284

commit v2 on v1

--- a/solution.py
+++ b/solution.py
@@ -102,8 +102,8 @@
             copy = send(sources[a], held.at[a, d - 1], (z_send, z_recv), (a, d), lines[d])
             copy.start()
             line_copies[a, d] = copy
-    for a in range(2):
-        for d in range(deep):
+    own_first = [(0, 0), (1, 0)] + [(a, d) for a in range(2) for d in range(1, deep)]
+    for a, d in own_first:
             if d:
                 line_copies[a, d].wait_recv()
             block = held[a, d - 1] if d else sources[a][...]

time: 148 us -> 146 us (0.986)
  Pallas kernels: 88.4 us -> 86.7 us
    pallas_call x1, Pallas kernels: 34.8 us -> 38.5 us  [combine(): pl.pallas_call(functools.partial(combine_kernel, experts, deep), out_shap...]
    pallas_call x1, Pallas kernels: 41.8 us -> 38.4 us  [dispatch(): pl.pallas_call(functools.partial(dispatch_kernel, experts, deep), out_sha...]
    pallas_call x1, Pallas kernels: 11.8 us -> 9.76 us  [closing(): pl.pallas_call(functools.partial(closing_kernel, count), out_shape=(jax.S...]
where the time goes in v2:
time: 146 us
  Pallas kernels  86.7 us (59%)
  matrix products  42.2 us (29%)
  local copies, waits for them, and re-layouts  9.39 us (6%)
  other arithmetic  5.45 us (4%)
  between operations  1.83 us (1%)
    pallas_call x1, Pallas kernels, combine(): pl.pallas_call(functools.partial(combine_kernel, experts, deep), out_shap...  38.5 us
    pallas_call x1, Pallas kernels, dispatch(): pl.pallas_call(functools.partial(dispatch_kernel, experts, deep), out_sha...  38.4 us
    pallas_call x1, Pallas kernels, closing(): pl.pallas_call(functools.partial(closing_kernel, count), out_shape=(jax.S...  9.76 us
    dot_general x1, matrix products, weight_grads(): lax.dot_general(slot_rows, d_up, major, preferred_element_type=jnp.float32)  7.39 us
    dot_general x1, matrix products, expert_work(): gate_act = jnp.dot(slot_rows, w_gate, preferred_element_type=jnp.float32)  6.84 us
    unnamed x53, local copies, waits for them, and re-layouts  6.42 us
    dot_general x1, matrix products, weight_grads(): lax.dot_general(slot_rows, d_gate, major, preferred_element_type=jnp.floa...  4.85 us
    dot_general x1, matrix products, weight_grads(): lax.dot_general(hidden, slot_cot, major, preferred_element_type=jnp.float32)  4.6 us

profile of v2, /device:TPU:0, one launch (start us, length us, event | category | flops | bytes accessed | tf_op | source)
XLA Modules:
  0.0 145.6 jit_solution(12163601371138688153)
XLA Ops:
  0.6 0.9 copy.102
  1.7 1.2 reduce-window.6
  4.5 1.0 select_reduce_fusion
  5.7 0.9 copy-done.2
  6.6 0.9 copy-done.4
  7.5 38.4 %shard_map.190 = (bf16[4,160,2048]{2,1,0:T(8,128)(2,1)S(1)}, bf16[4,160,2048]{2,1,0:T(8,128)(2,1)S(1)}) custom-call(bf16[256,256]{1,0:T(8,128)(2,1)S(1)} %copy-done.4, bf16[256,256]{1,0:T(8,128)(2,1)S(1)} %copy-done.2, bf16[4,160,256]{2,1,0:T(8,128)(2,1)S(1)} %bitcast.106, f32[4,160,1]{2,1,0:T(8,128)S(1)} %reshape.173.slot_weight), custom_call_target="tpu_custom_call" | custom-call | tf_op jit(solution)/shard_map/pallas_call | solution.py:153
  46.0 6.8 %fusion.2 = f32[640,896]{1,0:T(8,128)S(1)} fusion(bf16[640,2048]{1,0:T(8,128)(2,1)S(1)} %bitcast.112, bf16[1,2048,896]{2,1,0:T(8,128)(2,1)} %param.19), kind=kOutput, calls=%fused_computation.3 | convolution fusion | flops 2348810240 | bytes 8585216 | tf_op jit(solution)/shard_map/dot_general | solution.py:331
  52.9 2.9 %fusion.6 = f32[640,896]{1,0:T(8,128)S(1)} fusion(bf16[640,2048]{1,0:T(8,128)(2,1)S(1)} %bitcast.113, bf16[1,2048,896]{2,1,0:T(8,128)(2,1)S(1)} %copy-done.15), kind=kOutput, calls=%fused_computation.7 | convolution fusion | flops 2348810240 | bytes 8585216 | tf_op jit(solution)/shard_map/dot_general | solution.py:332
  55.8 3.6 %multiply_convert_fusion.1 = (bf16[640,896]{1,0:T(8,128)(2,1)S(1)}, bf16[640,896]{1,0:T(8,128)(2,1)S(1)}) fusion(f32[640,896]{1,0:T(8,128)S(1)} %fusion.2, f32[640,896]{1,0:T(8,128)S(1)} %fusion.6, bf16[640,2048]{1,0:T(8,128)(2,1)S(1)} %bitcast.110, bf16[1,896,2048]{2,1,0:T(8,128)(2,1)S(1)} %copy-done.13), kind=kOutput, calls=%fused_computation.16 | convolution fusion | flops 2356264960 | bytes 13172736 | tf_op jit(solution)/shard_map/dot_general | solution.py:336
  59.4 2.9 %fusion = f32[640,2048]{1,0:T(8,128)S(1)} fusion(bf16[640,896]{1,0:T(8,128)(2,1)S(1)} %get-tuple-element.45, bf16[1,2048,896]{2,1,0:T(8,128)(2,1)S(1)} %copy-done.14), kind=kOutput, calls=%fused_computation.1 | convolution fusion | flops 2348810240 | bytes 10059776 | tf_op jit(solution)/shard_map/dot_general | solution.py:341
  62.4 4.4 %add_convert_fusion = bf16[640,2048]{1,0:T(8,128)(2,1)} fusion(f32[640,2048]{1,0:T(8,128)S(1)} %fusion, bf16[640,896]{1,0:T(8,128)(2,1)S(1)} %get-tuple-element.44, bf16[1,2048,896]{2,1,0:T(8,128)(2,1)S(1)} %copy-done.15), kind=kOutput, calls=%fused_computation | convolution fusion | flops 2351431680 | bytes 12681216 | tf_op jit(solution)/shard_map/dot_general | solution.py:342
  67.0 1.7 %copy-done.1 = bf16[640,2048]{1,0:T(8,128)(2,1)S(1)} copy-done((bf16[640,2048]{1,0:T(8,128)(2,1)S(1)}, bf16[640,2048]{1,0:T(8,128)(2,1)}, u32[]{:S(2)}) %copy-start.1) | copy-done | bytes 2621464
  68.8 38.5 %shard_map.191 = bf16[256,2048]{1,0:T(8,128)(2,1)S(1)} custom-call(bf16[4,160,2048]{2,1,0:T(8,128)(2,1)S(1)} %bitcast.108, bf16[256,256]{1,0:T(8,128)(2,1)S(1)} %copy-done.3, bf16[4,256,160]{2,1,0:T(8,128)(2,1)S(1)} %bitcast.109), custom_call_target="tpu_custom_call" | custom-call | tf_op jit(solution)/shard_map/pallas_call | solution.py:269
  107.3 1.0 fusion.18
  108.4 1.0 fusion.16
  109.5 0.8 fusion.61
  114.1 9.8 %shard_map.192 = (f32[4,2,128]{2,1,0:T(2,128)S(1)}, bf16[4,128,512]{2,1,0:T(8,128)(2,1)S(1)}) custom-call(f32[2,128]{1,0:T(2,128)S(1)} %pad_maximum_fusion.13.summary, bf16[128,2048]{1,0:T(8,128)(2,1)S(1)} %convolution_convert_fusion.product), custom_call_target="tpu_custom_call" | custom-call | tf_op jit(solution)/shard_map/pallas_call | solution.py:314
  124.2 0.9 fusion.52
  125.4 0.9 fusion.49
  126.4 0.7 copy.127
  127.1 0.8 convert_reduce_fusion.1
  128.7 7.4 %convert_bitcast_fusion.1 = bf16[1,2048,896]{2,1,0:T(8,128)(2,1)} fusion(bf16[640,2048]{1,0:T(8,128)(2,1)} %bitcast.114, bf16[640,896]{1,0:T(8,128)(2,1)} %copy-done.22), kind=kOutput, calls=%fused_computation.12 | convolution fusion | flops 2350645248 | bytes 7438336 | tf_op jit(solution)/shard_map/dot_general | solution.py:351
  136.1 4.9 %convert_bitcast_fusion.2 = bf16[1,2048,896]{2,1,0:T(8,128)(2,1)} fusion(bf16[640,2048]{1,0:T(8,128)(2,1)S(1)} %bitcast.115, bf16[640,896]{1,0:T(8,128)(2,1)S(1)} %copy-done.17), kind=kOutput, calls=%fused_computation.13 | convolution fusion | flops 2350645248 | bytes 7438336 | tf_op jit(solution)/shard_map/dot_general | solution.py:348
  140.9 4.6 %convert_bitcast_fusion = bf16[1,896,2048]{2,1,0:T(8,128)(2,1)} fusion(bf16[640,2048]{1,0:T(8,128)(2,1)S(1)} %bitcast.111, f32[640,896]{1,0:T(8,128)S(1)} %copy-done.21, f32[640,896]{1,0:T(8,128)S(1)} %copy-done.19), kind=kOutput, calls=%fused_computation.11 | convolution fusion | flops 2354085888 | bytes 10878976 | tf_op jit(solution)/shard_map/dot_general | solution.py:354
  (207 shorter events, 6.9 us)
Async XLA Ops:
  0.6 110.1 %copy-start = (bf16[128,2048]{1,0:T(8,128)(2,1)S(1)}, bf16[128,2048]{1,0:T(8,128)(2,1)}, u32[]{:S(2)}) copy-start(bf16[128,2048]{1,0:T(8,128)(2,1)} %param.22) | copy-start | bytes 1572868
  5.7 0.9 copy-start.2
  6.6 0.9 copy-start.4
  46.0 6.9 %copy-start.7 = (bf16[4,160,2048]{2,1,0:T(8,128)(2,1)}, bf16[4,160,2048]{2,1,0:T(8,128)(2,1)S(1)}, u32[]{:S(2)}) copy-start(bf16[4,160,2048]{2,1,0:T(8,128)(2,1)S(1)} %get-tuple-element.10) | copy-start | bytes 7864324
  46.0 9.8 %copy-start.5 = (bf16[4,160,2048]{2,1,0:T(8,128)(2,1)}, bf16[4,160,2048]{2,1,0:T(8,128)(2,1)S(1)}, u32[]{:S(2)}) copy-start(bf16[4,160,2048]{2,1,0:T(8,128)(2,1)S(1)} %get-tuple-element.11) | copy-start | bytes 7864324
  46.0 6.9 %copy-start.15 = (bf16[1,2048,896]{2,1,0:T(8,128)(2,1)S(1)}, bf16[1,2048,896]{2,1,0:T(8,128)(2,1)}, u32[]{:S(2)}) copy-start(bf16[1,2048,896]{2,1,0:T(8,128)(2,1)} %param.20) | copy-start | bytes 11010052
  52.9 2.9 %copy-start.18 = (f32[640,896]{1,0:T(8,128)}, f32[640,896]{1,0:T(8,128)S(1)}, u32[]{:S(2)}) copy-start(f32[640,896]{1,0:T(8,128)S(1)} %fusion.2) | copy-start | bytes 6881284
  52.9 2.9 %copy-start.13 = (bf16[1,896,2048]{2,1,0:T(8,128)(2,1)S(1)}, bf16[1,896,2048]{2,1,0:T(8,128)(2,1)}, u32[]{:S(2)}) copy-start(bf16[1,896,2048]{2,1,0:T(8,128)(2,1)} %param.21) | copy-start | bytes 11010052
  55.8 3.6 %copy-start.20 = (f32[640,896]{1,0:T(8,128)}, f32[640,896]{1,0:T(8,128)S(1)}, u32[]{:S(2)}) copy-start(f32[640,896]{1,0:T(8,128)S(1)} %fusion.6) | copy-start | bytes 6881284
  55.8 3.6 %copy-start.14 = (bf16[1,2048,896]{2,1,0:T(8,128)(2,1)S(1)}, bf16[1,2048,896]{2,1,0:T(8,128)(2,1)}, u32[]{:S(2)}) copy-start(bf16[1,2048,896]{2,1,0:T(8,128)(2,1)} %param.19) | copy-start | bytes 11010052
  59.4 3.0 %copy-start.16 = (bf16[640,896]{1,0:T(8,128)(2,1)}, bf16[640,896]{1,0:T(8,128)(2,1)S(1)}, u32[]{:S(2)}) copy-start(bf16[640,896]{1,0:T(8,128)(2,1)S(1)} %get-tuple-element.45) | copy-start | bytes 3440644
  59.4 2.9 %copy-start.22 = (bf16[640,896]{1,0:T(8,128)(2,1)}, bf16[640,896]{1,0:T(8,128)(2,1)S(1)}, u32[]{:S(2)}) copy-start(bf16[640,896]{1,0:T(8,128)(2,1)S(1)} %get-tuple-element.44) | copy-start | bytes 3440644
  62.4 4.6 %copy-start.3 = (bf16[256,256]{1,0:T(8,128)(2,1)S(1)}, bf16[256,256]{1,0:T(8,128)(2,1)}, u32[]{:S(2)}) copy-start(bf16[256,256]{1,0:T(8,128)(2,1)} %cot_in.3) | copy-start | bytes 393220
  67.0 1.7 %copy-start.1 = (bf16[640,2048]{1,0:T(8,128)(2,1)S(1)}, bf16[640,2048]{1,0:T(8,128)(2,1)}, u32[]{:S(2)}) copy-start(bf16[640,2048]{1,0:T(8,128)(2,1)} %add_convert_fusion) | copy-start | bytes 7864324
  68.7 38.5 %copy-start.11 = (bf16[128,256]{1,0:T(8,128)(2,1)S(1)}, bf16[128,256]{1,0:T(8,128)(2,1)}, u32[]{:S(2)}) copy-start(bf16[128,256]{1,0:T(8,128)(2,1)} %param.23) | copy-start | bytes 196612
  68.7 41.5 %copy-start.10 = (bf16[128,256]{1,0:T(8,128)(2,1)S(1)}, bf16[128,256]{1,0:T(8,128)(2,1)}, u32[]{:S(2)}) copy-start(bf16[128,256]{1,0:T(8,128)(2,1)} %param.25) | copy-start | bytes 196612
  68.7 41.8 %copy-start.12 = (bf16[128,256]{1,0:T(8,128)(2,1)S(1)}, bf16[128,256]{1,0:T(8,128)(2,1)}, u32[]{:S(2)}) copy-start(bf16[128,256]{1,0:T(8,128)(2,1)} %param.24) | copy-start | bytes 196612
  68.7 41.9 %copy-start.9 = (f32[128,256]{1,0:T(8,128)S(1)}, f32[128,256]{1,0:T(8,128)}, u32[]{:S(2)}) copy-start(f32[128,256]{1,0:T(8,128)} %param.29) | copy-start | bytes 393220
  128.7 7.4 %copy-start.8 = (bf16[4,160,2048]{2,1,0:T(8,128)(2,1)S(1)}, bf16[4,160,2048]{2,1,0:T(8,128)(2,1)}, u32[]{:S(2)}) copy-start(bf16[4,160,2048]{2,1,0:T(8,128)(2,1)} %copy-done.7) | copy-start | bytes 7864324
  128.7 7.4 %copy-start.17 = (bf16[640,896]{1,0:T(8,128)(2,1)S(1)}, bf16[640,896]{1,0:T(8,128)(2,1)}, u32[]{:S(2)}) copy-start(bf16[640,896]{1,0:T(8,128)(2,1)} %copy-done.16) | copy-start | bytes 3440644
  136.1 4.9 %copy-start.6 = (bf16[4,160,2048]{2,1,0:T(8,128)(2,1)S(1)}, bf16[4,160,2048]{2,1,0:T(8,128)(2,1)}, u32[]{:S(2)}) copy-start(bf16[4,160,2048]{2,1,0:T(8,128)(2,1)} %copy-done.5) | copy-start | bytes 7864324
  136.1 4.9 %copy-start.19 = (f32[640,896]{1,0:T(8,128)S(1)}, f32[640,896]{1,0:T(8,128)}, u32[]{:S(2)}) copy-start(f32[640,896]{1,0:T(8,128)} %copy-done.18) | copy-start | bytes 6881284
  136.1 4.9 %copy-start.21 = (f32[640,896]{1,0:T(8,128)S(1)}, f32[640,896]{1,0:T(8,128)}, u32[]{:S(2)}) copy-start(f32[640,896]{1,0:T(8,128)} %copy-done.20) | copy-start | bytes 6881284
